TPU v7x, 32 devices: a whole 2x2x4 slice. The times are simulated.
32 devices in a mesh: fs: 8 (over z, x), tp: 4 (over y, core).
Axes of the slice: x: 2, y: 2, z: 4, core: 2. Of those that a mesh axis runs over, the one named last changes fastest.
Arguments:
- tokens: bfloat16 [16, 384, 2048], P('fs', None, 'tp'), may hold values from -20 to 20
- first_gain: float32 [2048], replicated, may hold values from 0.1 to 1.9
- first_gate: bfloat16 [2048, 5120], P('fs', 'tp'), may hold values from -0.125 to 0.125
- first_up: bfloat16 [2048, 5120], P('fs', 'tp'), may hold values from -0.125 to 0.125
- first_down: bfloat16 [5120, 2048], P('tp', 'fs'), may hold values from -0.078125 to 0.078125
- mixer_gain: float32 [2048], replicated, may hold values from 0.1 to 1.9
- conv_input: bfloat16 [2048, 1024], P('fs', 'tp'), may hold values from -0.125 to 0.125
- outer_gate: bfloat16 [2048, 1024], P('fs', 'tp'), may hold values from -0.125 to 0.125
- inner_gate: bfloat16 [2048, 1024], P('fs', 'tp'), may hold values from -0.125 to 0.125
- conv_taps: float32 [3, 1024], P(None, 'tp'), may hold values from -3.5 to 3.5
- mixer_out: bfloat16 [1024, 2048], P('tp', 'fs'), may hold values from -0.1875 to 0.1875
- second_gain: float32 [2048], replicated, may hold values from 0.1 to 1.9
- second_gate: bfloat16 [2048, 5120], P('fs', 'tp'), may hold values from -0.125 to 0.125
- second_up: bfloat16 [2048, 5120], P('fs', 'tp'), may hold values from -0.125 to 0.125
- second_down: bfloat16 [5120, 2048], P('tp', 'fs'), may hold values from -0.078125 to 0.078125
Outputs:
- layer_out: bfloat16 [16, 384, 2048], P('fs', None, 'tp')
All inputs are finite; a program needn't handle non-finite values.
Results may differ from a plain program's by a relative error of at most 0.015.
Values may be sent and summed in bfloat16 or wider, within the bound.
A program may use at most 64 MiB of HBM per device.

v0:
```python
import jax
import jax.numpy as jnp
from jax import lax
from jax.sharding import PartitionSpec as P

epsilon = 1e-05


def norm_rows(stream, gain):
    whole = lax.all_gather(stream, "tp", axis=1, tiled=True)
    values = whole.astype(jnp.float32)
    scale = lax.rsqrt(jnp.mean(values * values, axis=1, keepdims=True) + epsilon)
    return (values * scale * gain).astype(jnp.bfloat16)


def add_rows(gathered, piece):
    return jnp.dot(gathered, piece, preferred_element_type=jnp.float32)


def ffn_inputs(gathered, gate_weight, up_weight):
    empty = jnp.zeros((gathered.shape[0], gate_weight.shape[1]), jnp.float32)

    def add_single(total, piece, start):
        return add_rows(gathered, piece)

    gate = add_single(empty, lax.all_gather(gate_weight, "fs", axis=0, tiled=True), jnp.int32(0))
    upward = add_single(empty, lax.all_gather(up_weight, "fs", axis=0, tiled=True), jnp.int32(0))
    return (gate, upward)


def mixer_inputs(gathered, conv_input, outer_gate, inner_gate):
    empty = jnp.zeros((gathered.shape[0], conv_input.shape[1]), jnp.float32)

    def add_single(total, piece, start):
        return add_rows(gathered, piece)

    conv_values = add_single(
        empty, lax.all_gather(conv_input, "fs", axis=0, tiled=True), jnp.int32(0)
    )
    outer = add_single(empty, lax.all_gather(outer_gate, "fs", axis=0, tiled=True), jnp.int32(0))
    inner = add_single(empty, lax.all_gather(inner_gate, "fs", axis=0, tiled=True), jnp.int32(0))
    return (conv_values, outer, inner)


def project_down(hidden, weight):
    partial_sum = jnp.dot(
        hidden, lax.all_gather(weight, "fs", axis=1, tiled=True), preferred_element_type=jnp.float32
    )
    result = lax.psum_scatter(
        partial_sum.astype(jnp.bfloat16), "tp", scatter_dimension=1, tiled=True
    ).astype(jnp.float32)
    return result


def half_ffn(stream, gain, gate_weight, up_weight, down_weight):
    gathered = norm_rows(stream, gain)
    gate, upward = ffn_inputs(gathered, gate_weight, up_weight)
    hidden = (jax.nn.silu(gate) * upward).astype(jnp.bfloat16)
    branch = project_down(hidden, down_weight)
    return (stream.astype(jnp.float32) + 0.5 * branch).astype(jnp.bfloat16)


def conv_mixer(stream, seqs, gain, conv_input, outer_gate, inner_gate, conv_taps, mixer_out):
    gathered = norm_rows(stream, gain)
    conv_values, outer, inner = mixer_inputs(gathered, conv_input, outer_gate, inner_gate)
    gated_input = (inner * conv_values).reshape(seqs, -1, conv_values.shape[1])
    one_back = jnp.pad(gated_input, ((0, 0), (1, 0), (0, 0)))[:, :-1]
    two_back = jnp.pad(gated_input, ((0, 0), (2, 0), (0, 0)))[:, :-2]
    convolved = conv_taps[0] * two_back + conv_taps[1] * one_back + conv_taps[2] * gated_input
    mixed = (outer * convolved.reshape(conv_values.shape)).astype(jnp.bfloat16)
    branch = project_down(mixed, mixer_out)
    return (stream.astype(jnp.float32) + branch).astype(jnp.bfloat16)


def on_device(
    tokens,
    first_gain,
    first_gate,
    first_up,
    first_down,
    mixer_gain,
    conv_input,
    outer_gate,
    inner_gate,
    conv_taps,
    mixer_out,
    second_gain,
    second_gate,
    second_up,
    second_down,
):
    seqs, length, width = tokens.shape
    stream = tokens.reshape(seqs * length, width)
    stream = half_ffn(stream, first_gain, first_gate, first_up, first_down)
    stream = conv_mixer(
        stream, seqs, mixer_gain, conv_input, outer_gate, inner_gate, conv_taps, mixer_out
    )
    stream = half_ffn(stream, second_gain, second_gate, second_up, second_down)
    return stream.reshape(seqs, length, width)


def solution(mesh):
    in_specs = (
        P("fs", None, "tp"),
        P(),
        P("fs", "tp"),
        P("fs", "tp"),
        P("tp", "fs"),
        P(),
        P("fs", "tp"),
        P("fs", "tp"),
        P("fs", "tp"),
        P(None, "tp"),
        P("tp", "fs"),
        P(),
        P("fs", "tp"),
        P("fs", "tp"),
        P("tp", "fs"),
    )
    out_specs = P("fs", None, "tp")
    return jax.shard_map(
        on_device, mesh=mesh, in_specs=in_specs, out_specs=out_specs, check_vma=False
    )
```

profile of v0, /device:TPU:0, one launch (start us, length us, event | category | flops | bytes accessed | tf_op | source)
XLA Modules:
  0.0 947.5 jit_solution(4137865059658070734)
XLA Ops:
  6.5 0.7 all-gather.14.cloned.1.call-update
  7.3 0.0 all-gather.16.cloned.1.call-start
  7.3 0.7 all-gather.16.cloned.1.call-update
  8.0 0.0 all-gather.18.cloned.1.call-start
  8.1 0.7 all-gather.18.cloned.1.call-update
  8.7 0.0 all-gather.20.cloned.1.call-start
  8.8 0.5 all-gather.20.cloned.1.call-update
  9.3 0.0 reduce-scatter.4.cloned.1.call-start
  9.4 30.8 %all-gather.14.cloned.1.call-done = bf16[768,2048]{1,0:T(8,128)(2,1)} async-done(((bf16[768,512]{1,0:T(8,128)(2,1)}), bf16[768,2048]{1,0:T(8,128)(2,1)}) %all-gather.14.cloned.1.call-update) | async-done | bytes 3145744 | tf_op jit(solution)/shard_map/all_gather | solution.py:10
  40.2 2.6 fusion
  42.8 85.5 %all-gather.16.cloned.1.call-done = bf16[2048,1280]{1,0:T(8,128)(2,1)} async-done(((bf16[256,1280]{1,0:T(8,128)(2,1)}), bf16[2048,1280]{1,0:T(8,128)(2,1)}) %all-gather.16.cloned.1.call-update) | async-done | bytes 5242896 | tf_op jit(solution)/shard_map/all_gather | solution.py:26
  128.3 9.6 %fusion.18 = f32[768,1280]{1,0:T(8,128)} fusion(bf16[2048,1280]{1,0:T(8,128)(2,1)} %all-gather.16.cloned.1.call-done, bf16[768,2048]{1,0:T(8,128)(2,1)} %all-gather.14.cloned.1.call-done, f32[2048]{0:T(1024)S(1)} %copy-done.5, f32[768]{0:T(1024)S(1)} %add_rsqrt_fusion.2), kind=kOutput, calls=%fused_computation.29 | convolution fusion | flops 4032823296 | bytes 12332032 | tf_op jit(solution)/shard_map/dot_general | solution.py:17
  137.8 76.7 %all-gather.18.cloned.1.call-done = bf16[2048,1280]{1,0:T(8,128)(2,1)} async-done(((bf16[256,1280]{1,0:T(8,128)(2,1)}), bf16[2048,1280]{1,0:T(8,128)(2,1)}) %all-gather.18.cloned.1.call-update) | async-done | bytes 5242896 | tf_op jit(solution)/shard_map/all_gather | solution.py:27
  214.5 86.9 %all-gather.20.cloned.1.call-done = bf16[1280,2048]{1,0:T(8,128)(2,1)} async-done(((bf16[1280,256]{1,0:T(8,128)(2,1)}), bf16[1280,2048]{1,0:T(8,128)(2,1)}) %all-gather.20.cloned.1.call-update) | async-done | bytes 5242896 | tf_op jit(solution)/shard_map/all_gather | solution.py:47
  301.4 16.4 %convolution_convert_fusion.2 = bf16[768,2048]{1,0:T(8,128)(2,1)} fusion(bf16[1280,2048]{1,0:T(8,128)(2,1)} %all-gather.20.cloned.1.call-done, bf16[2048,1280]{1,0:T(8,128)(2,1)} %all-gather.18.cloned.1.call-done, f32[768,1280]{1,0:T(8,128)} %fusion.18, bf16[768,2048]{1,0:T(8,128)(2,1)S(1)} %copy-done.3, f32[2048]{0:T(1024)S(1)} %copy-done.5, ...), kind=kOutput, calls=%fused_computation.21 | convolution fusion | flops 8066826240 | bytes 20720640 | tf_op jit(solution)/shard_map/dot_general | solution.py:46
  317.8 0.0 reduce-scatter.4.cloned.1.call-update
  317.9 0.0 copy-start.6
  317.9 0.0 all-gather.22.cloned.1.call-start
  317.9 36.0 %reduce-scatter.4.cloned.1.call-done = bf16[768,512]{1,0:T(8,128)(2,1)} async-done(((bf16[768,2048]{1,0:T(8,128)(2,1)}), bf16[768,512]{1,0:T(8,128)(2,1)}) %reduce-scatter.4.cloned.1.call-update) | async-done | bytes 786448 | tf_op jit(solution)/shard_map/reduce_scatter | solution.py:49
  353.9 2.5 add_convert_fusion.2
  356.4 0.0 all-gather.22.cloned.1.call-update
  356.4 0.0 all-gather.26.cloned.1.call-start
  356.5 0.7 all-gather.26.cloned.1.call-update
  357.2 0.0 all-gather.28.cloned.1.call-start
  357.2 0.7 all-gather.28.cloned.1.call-update
  357.9 0.0 all-gather.24.cloned.1.call-start
  358.0 0.7 all-gather.24.cloned.1.call-update
  358.7 0.0 all-gather.30.cloned.1.call-start
  358.7 0.5 all-gather.30.cloned.1.call-update
  359.2 0.2 reduce-scatter.6.cloned.1.call-start
  359.5 25.6 %all-gather.22.cloned.1.call-done = bf16[768,2048]{1,0:T(8,128)(2,1)} async-done(((bf16[768,512]{1,0:T(8,128)(2,1)}), bf16[768,2048]{1,0:T(8,128)(2,1)}) %all-gather.22.cloned.1.call-update) | async-done | bytes 3145744 | tf_op jit(solution)/shard_map/all_gather | solution.py:10
  385.1 2.6 fusion.3
  387.7 39.8 %all-gather.26.cloned.1.call-done = bf16[2048,256]{1,0:T(8,128)(2,1)} async-done(((bf16[256,256]{1,0:T(8,128)(2,1)}), bf16[2048,256]{1,0:T(8,128)(2,1)}) %all-gather.26.cloned.1.call-update) | async-done | bytes 1048592 | tf_op jit(solution)/shard_map/all_gather | solution.py:41
  427.5 4.1 fusion.29
  431.6 37.0 %all-gather.28.cloned.1.call-done = bf16[2048,256]{1,0:T(8,128)(2,1)} async-done(((bf16[256,256]{1,0:T(8,128)(2,1)}), bf16[2048,256]{1,0:T(8,128)(2,1)}) %all-gather.28.cloned.1.call-update) | async-done | bytes 1048592 | tf_op jit(solution)/shard_map/all_gather | solution.py:38
  468.7 0.0 copy-done.2
  468.7 2.5 convolution_multiply_fusion.2
  471.1 0.2 fusion.24
  471.4 38.4 %all-gather.24.cloned.1.call-done = bf16[2048,256]{1,0:T(8,128)(2,1)} async-done(((bf16[256,256]{1,0:T(8,128)(2,1)}), bf16[2048,256]{1,0:T(8,128)(2,1)}) %all-gather.24.cloned.1.call-update) | async-done | bytes 1048592 | tf_op jit(solution)/shard_map/all_gather | solution.py:40
  509.8 40.0 %all-gather.30.cloned.1.call-done = bf16[256,2048]{1,0:T(8,128)(2,1)} async-done(((bf16[256,256]{1,0:T(8,128)(2,1)}), bf16[256,2048]{1,0:T(8,128)(2,1)}) %all-gather.30.cloned.1.call-update) | async-done | bytes 1048592 | tf_op jit(solution)/shard_map/all_gather | solution.py:47
  549.8 7.6 convolution_convert_fusion
  557.5 0.0 reduce-scatter.6.cloned.1.call-update
  557.5 0.0 copy-start.7
  557.5 0.0 all-gather.32.cloned.1.call-start
  557.5 36.8 %reduce-scatter.6.cloned.1.call-done = bf16[768,512]{1,0:T(8,128)(2,1)} async-done(((bf16[768,2048]{1,0:T(8,128)(2,1)}), bf16[768,512]{1,0:T(8,128)(2,1)}) %reduce-scatter.6.cloned.1.call-update) | async-done | bytes 786448 | tf_op jit(solution)/shard_map/reduce_scatter | solution.py:49
  594.4 2.2 add_convert_fusion.1
  596.6 0.0 all-gather.32.cloned.1.call-update
  596.6 0.0 all-gather.34.cloned.1.call-start
  596.7 0.7 all-gather.34.cloned.1.call-update
  597.4 0.0 all-gather.36.cloned.1.call-start
  597.4 0.5 all-gather.36.cloned.1.call-update
  598.0 0.0 all-gather.38.cloned.1.call-start
  598.0 0.5 all-gather.38.cloned.1.call-update
  598.5 0.3 reduce-scatter.8.cloned.1.call-start
  598.8 26.5 %all-gather.32.cloned.1.call-done = bf16[768,2048]{1,0:T(8,128)(2,1)} async-done(((bf16[768,512]{1,0:T(8,128)(2,1)}), bf16[768,2048]{1,0:T(8,128)(2,1)}) %all-gather.32.cloned.1.call-update) | async-done | bytes 3145744 | tf_op jit(solution)/shard_map/all_gather | solution.py:10
  625.3 2.6 fusion.6
  627.9 85.5 %all-gather.34.cloned.1.call-done = bf16[2048,1280]{1,0:T(8,128)(2,1)} async-done(((bf16[256,1280]{1,0:T(8,128)(2,1)}), bf16[2048,1280]{1,0:T(8,128)(2,1)}) %all-gather.34.cloned.1.call-update) | async-done | bytes 5242896 | tf_op jit(solution)/shard_map/all_gather | solution.py:26
  713.4 9.6 %fusion.13 = f32[768,1280]{1,0:T(8,128)} fusion(bf16[2048,1280]{1,0:T(8,128)(2,1)} %all-gather.34.cloned.1.call-done, bf16[768,2048]{1,0:T(8,128)(2,1)} %all-gather.32.cloned.1.call-done, f32[2048]{0:T(1024)S(1)} %copy-done.7, f32[768]{0:T(1024)S(1)} %add_rsqrt_fusion), kind=kOutput, calls=%fused_computation.28 | convolution fusion | flops 4032823296 | bytes 12332032 | tf_op jit(solution)/shard_map/dot_general | solution.py:17
  723.0 76.5 %all-gather.36.cloned.1.call-done = bf16[2048,1280]{1,0:T(8,128)(2,1)} async-done(((bf16[256,1280]{1,0:T(8,128)(2,1)}), bf16[2048,1280]{1,0:T(8,128)(2,1)}) %all-gather.36.cloned.1.call-update) | async-done | bytes 5242896 | tf_op jit(solution)/shard_map/all_gather | solution.py:27
  799.5 86.9 %all-gather.38.cloned.1.call-done = bf16[1280,2048]{1,0:T(8,128)(2,1)} async-done(((bf16[1280,256]{1,0:T(8,128)(2,1)}), bf16[1280,2048]{1,0:T(8,128)(2,1)}) %all-gather.38.cloned.1.call-update) | async-done | bytes 5242896 | tf_op jit(solution)/shard_map/all_gather | solution.py:47
  886.4 16.2 %convolution_convert_fusion.1 = bf16[768,2048]{1,0:T(8,128)(2,1)} fusion(bf16[1280,2048]{1,0:T(8,128)(2,1)} %all-gather.38.cloned.1.call-done, bf16[2048,1280]{1,0:T(8,128)(2,1)} %all-gather.36.cloned.1.call-done, f32[768,1280]{1,0:T(8,128)} %fusion.13, bf16[768,2048]{1,0:T(8,128)(2,1)} %all-gather.32.cloned.1.call-done, f32[2048]{0:T(1024)S(1)} %copy-done.7, ...), kind=kOutput, calls=%fused_computation.20 | convolution fusion | flops 8066826240 | bytes 20720640 | tf_op jit(solution)/shard_map/dot_general | solution.py:46
  902.6 0.0 reduce-scatter.8.cloned.1.call-update
  902.6 36.1 %reduce-scatter.8.cloned.1.call-done = bf16[768,512]{1,0:T(8,128)(2,1)} async-done(((bf16[768,2048]{1,0:T(8,128)(2,1)}), bf16[768,512]{1,0:T(8,128)(2,1)}) %reduce-scatter.8.cloned.1.call-update) | async-done | bytes 786448 | tf_op jit(solution)/shard_map/reduce_scatter | solution.py:49
  938.7 2.2 add_convert_fusion
  (18 shorter events, 0.1 us)
Async XLA Ops:
  6.5 121.7 %copy-start.5 = (f32[2048]{0:T(1024)S(1)}, f32[2048]{0:T(1024)}, u32[]{:S(2)}) copy-start(f32[2048]{0:T(1024)} %param.16) | copy-start | bytes 24580
  6.5 33.6 %all-gather.14.cloned.1.call-start = ((), (), s32[]{:S(2)}) async-start(), calls=%async_computation.3 | async-start | bytes 3932160 | tf_op jit(solution)/shard_map/all_gather | solution.py:10
  7.3 121.0 %all-gather.16.cloned.1.call-start = ((), (), s32[]{:S(2)}) async-start(), calls=%async_computation.4 | async-start | bytes 5898240 | tf_op jit(solution)/shard_map/all_gather | solution.py:26
  8.0 206.5 %all-gather.18.cloned.1.call-start = ((), (), s32[]{:S(2)}) async-start(), calls=%async_computation.5 | async-start | bytes 5898240 | tf_op jit(solution)/shard_map/all_gather | solution.py:27
  8.7 292.7 %all-gather.20.cloned.1.call-start = ((), (), s32[]{:S(2)}) async-start(), calls=%async_computation.6 | async-start | bytes 5898240 | tf_op jit(solution)/shard_map/all_gather | solution.py:47
  9.3 344.6 %reduce-scatter.4.cloned.1.call-start = ((), (), s32[]{:S(2)}) async-start(), calls=%async_computation.7 | async-start | bytes 3932160 | tf_op jit(solution)/shard_map/reduce_scatter | solution.py:49
  42.7 258.7 %copy-start.3 = (bf16[768,2048]{1,0:T(8,128)(2,1)S(1)}, bf16[768,2048]{1,0:T(8,128)(2,1)}, u32[]{:S(2)}) copy-start(bf16[768,2048]{1,0:T(8,128)(2,1)} %all-gather.14.cloned.1.call-done) | copy-start | bytes 9437188
  317.8 41.6 %copy-start.4 = (f32[3,256]{1,0:T(4,128)S(1)}, f32[3,256]{1,0:T(4,128)}, u32[]{:S(2)}) copy-start(f32[3,256]{1,0:T(4,128)} %param.24) | copy-start | bytes 9220
  317.9 109.6 %copy-start.6 = (f32[2048]{0:T(1024)S(1)}, f32[2048]{0:T(1024)}, u32[]{:S(2)}) copy-start(f32[2048]{0:T(1024)} %param.20) | copy-start | bytes 24580
  317.9 67.2 %all-gather.22.cloned.1.call-start = ((), (), s32[]{:S(2)}) async-start(), calls=%async_computation.8 | async-start | bytes 3932160 | tf_op jit(solution)/shard_map/all_gather | solution.py:10
  356.4 71.1 %all-gather.26.cloned.1.call-start = ((), (), s32[]{:S(2)}) async-start(), calls=%async_computation.10 | async-start | bytes 1179648 | tf_op jit(solution)/shard_map/all_gather | solution.py:41
  357.2 111.5 %all-gather.28.cloned.1.call-start = ((), (), s32[]{:S(2)}) async-start(), calls=%async_computation.11 | async-start | bytes 1179648 | tf_op jit(solution)/shard_map/all_gather | solution.py:38
  357.9 151.9 %all-gather.24.cloned.1.call-start = ((), (), s32[]{:S(2)}) async-start(), calls=%async_computation.9 | async-start | bytes 1179648 | tf_op jit(solution)/shard_map/all_gather | solution.py:40
  358.7 191.2 %all-gather.30.cloned.1.call-start = ((), (), s32[]{:S(2)}) async-start(), calls=%async_computation.12 | async-start | bytes 1179648 | tf_op jit(solution)/shard_map/all_gather | solution.py:47
  359.2 235.1 %reduce-scatter.6.cloned.1.call-start = ((), (), s32[]{:S(2)}) async-start(), calls=%async_computation.13 | async-start | bytes 3932160 | tf_op jit(solution)/shard_map/reduce_scatter | solution.py:49
  387.7 81.0 %copy-start.2 = (bf16[768,2048]{1,0:T(8,128)(2,1)S(1)}, bf16[768,2048]{1,0:T(8,128)(2,1)}, u32[]{:S(2)}) copy-start(bf16[768,2048]{1,0:T(8,128)(2,1)} %all-gather.22.cloned.1.call-done) | copy-start | bytes 9437188
  549.8 44.5 %copy-start = (bf16[768,512]{1,0:T(8,128)(2,1)S(1)}, bf16[768,512]{1,0:T(8,128)(2,1)}, u32[]{:S(2)}) copy-start(bf16[768,512]{1,0:T(8,128)(2,1)} %add_convert_fusion.2) | copy-start | bytes 2359300
  557.5 155.9 %copy-start.7 = (f32[2048]{0:T(1024)S(1)}, f32[2048]{0:T(1024)}, u32[]{:S(2)}) copy-start(f32[2048]{0:T(1024)} %param.26) | copy-start | bytes 24580
  557.5 67.8 %all-gather.32.cloned.1.call-start = ((), (), s32[]{:S(2)}) async-start(), calls=%async_computation.14 | async-start | bytes 3932160 | tf_op jit(solution)/shard_map/all_gather | solution.py:10
  596.6 116.8 %all-gather.34.cloned.1.call-start = ((), (), s32[]{:S(2)}) async-start(), calls=%async_computation.15 | async-start | bytes 5898240 | tf_op jit(solution)/shard_map/all_gather | solution.py:26
  597.4 202.1 %all-gather.36.cloned.1.call-start = ((), (), s32[]{:S(2)}) async-start(), calls=%async_computation.16 | async-start | bytes 5898240 | tf_op jit(solution)/shard_map/all_gather | solution.py:27
  598.0 288.4 %all-gather.38.cloned.1.call-start = ((), (), s32[]{:S(2)}) async-start(), calls=%async_computation.17 | async-start | bytes 5898240 | tf_op jit(solution)/shard_map/all_gather | solution.py:47
  598.5 340.2 %reduce-scatter.8.cloned.1.call-start = ((), (), s32[]{:S(2)}) async-start(), calls=%async_computation.18 | async-start | bytes 3932160 | tf_op jit(solution)/shard_map/reduce_scatter | solution.py:49
  723.0 215.7 %copy-start.1 = (bf16[768,512]{1,0:T(8,128)(2,1)S(1)}, bf16[768,512]{1,0:T(8,128)(2,1)}, u32[]{:S(2)}) copy-start(bf16[768,512]{1,0:T(8,128)(2,1)} %add_convert_fusion.1) | copy-start | bytes 2359300
Sparse Core Ops, SparseCore 0:
  8.9 31.2 all-gather.13
  42.3 85.8 all-gather.15
  130.4 84.0 all-gather.17
  216.4 84.9 all-gather.19
  318.0 35.8 reduce-scatter.3
  356.5 28.4 all-gather.21
  387.2 40.2 all-gather.25
  429.6 38.9 all-gather.27
  470.8 38.9 all-gather.23
  511.7 38.0 all-gather.29
  557.6 36.7 reduce-scatter.5
  596.7 28.5 all-gather.31
  627.5 85.8 all-gather.33
  715.4 84.0 all-gather.35
  801.4 84.9 all-gather.37
  902.8 35.8 reduce-scatter.7
where the time goes:
time: 948 us; the launch traced here: 947 us
  waiting for transfers between devices  852 us (90%)
  matrix products  66 us (7%)
  other arithmetic  14.9 us (2%)
  between operations  13.4 us (1%)
    all_gather x3, waiting for transfers between devices, project_down(): lax.all_gather(weight, 'fs', axis=1, tiled=True)  214 us
    all_gather x2, waiting for transfers between devices, ffn_inputs(): lax.all_gather(gate_weight, 'fs', axis=0, tiled=True)  171 us
    all_gather x2, waiting for transfers between devices, ffn_inputs(): lax.all_gather(up_weight, 'fs', axis=0, tiled=True)  153 us
    reduce_scatter x3, waiting for transfers between devices, project_down(): lax.psum_scatter(partial_sum.astype(jnp.bfloat16), 'tp', scatter_dimensio...  109 us
    all_gather x3, waiting for transfers between devices, norm_rows(): whole = lax.all_gather(stream, 'tp', axis=1, tiled=True)  82.9 us
    dot_general x3, matrix products, project_down(): jnp.dot(hidden, lax.all_gather(weight, 'fs', axis=1, tiled=True), preferr...  40.2 us
    all_gather x1, waiting for transfers between devices, mixer_inputs(): lax.all_gather(inner_gate, 'fs', axis=0, tiled=True)  39.8 us
    all_gather x1, waiting for transfers between devices, mixer_inputs(): lax.all_gather(outer_gate, 'fs', axis=0, tiled=True)  38.4 us
  transfers between devices with their start and end apart: 16, of which 16 were waited for; matrix products, arithmetic and copies ran while one was open for 4% of the time, Pallas kernels for 0%

commit v1 on v0

--- a/solution.py
+++ b/solution.py
@@ -6,8 +6,23 @@
 epsilon = 1e-05
 
 
+def bring_the_point(inner_x):
+    mesh_dim = "tp"
+    n_dev_all = lax.axis_size(mesh_dim)
+    kept_rows = [inner_x]
+    for h in [*range(n_dev_all - 1)]:
+        kept_rows.append(
+            lax.ppermute(
+                kept_rows[-1], mesh_dim, [(nth, (nth + 1) % n_dev_all) for nth in range(n_dev_all)]
+            )
+        )
+    everything = jnp.concatenate(kept_rows[::-1], axis=1)
+    block_now = jnp.roll(everything, (lax.axis_index(mesh_dim) + 1) * inner_x.shape[1], axis=1)
+    return block_now
+
+
 def norm_rows(stream, gain):
-    whole = lax.all_gather(stream, "tp", axis=1, tiled=True)
+    whole = bring_the_point(stream)
     values = whole.astype(jnp.float32)
     scale = lax.rsqrt(jnp.mean(values * values, axis=1, keepdims=True) + epsilon)
     return (values * scale * gain).astype(jnp.bfloat16)

time: 948 us -> 855 us (0.902)
  waiting for transfers between devices: 852 us -> 742 us
  other arithmetic: 14.9 us -> 32.4 us
    ppermute x0 -> x9, waiting for transfers between devices: none -> 102 us  [bring_the_point(): lax.ppermute(kept_rows[-1], mesh_dim, [(nth, (nth + 1) % n_dev_all) for n...]
    all_gather x2, waiting for transfers between devices: 171 us -> 88 us  [ffn_inputs(): lax.all_gather(gate_weight, 'fs', axis=0, tiled=True)]
    all_gather x3 -> x0, waiting for transfers between devices: 82.9 us -> none  [norm_rows(): whole = lax.all_gather(stream, 'tp', axis=1, tiled=True)]
    all_gather x1, waiting for transfers between devices: 37 us -> 0.01 us  [mixer_inputs(): lax.all_gather(conv_input, 'fs', axis=0, tiled=True)]
    reduce_sum x3, other arithmetic: 7.71 us -> 27 us  [norm_rows(): jnp.mean(values * values, axis=1, keepdims=True) + epsilon]
  transfers between devices with their start and end apart: 16 -> 22, of which waited for: 16 -> 21; matrix products, arithmetic and copies ran while one was open for 4% -> 6% of each run, Pallas kernels for 0% -> 0%
where the time goes in v1:
time: 855 us
  waiting for transfers between devices  742 us (87%)
  matrix products  64.8 us (8%)
  other arithmetic  32.4 us (4%)
  between operations  13.4 us (2%)
    all_gather x3, waiting for transfers between devices, project_down(): lax.all_gather(weight, 'fs', axis=1, tiled=True)  214 us
    all_gather x2, waiting for transfers between devices, ffn_inputs(): lax.all_gather(up_weight, 'fs', axis=0, tiled=True)  154 us
    reduce_scatter x3, waiting for transfers between devices, project_down(): lax.psum_scatter(partial_sum.astype(jnp.bfloat16), 'tp', scatter_dimensio...  106 us
    ppermute x9, waiting for transfers between devices, bring_the_point(): lax.ppermute(kept_rows[-1], mesh_dim, [(nth, (nth + 1) % n_dev_all) for n...  102 us
    all_gather x2, waiting for transfers between devices, ffn_inputs(): lax.all_gather(gate_weight, 'fs', axis=0, tiled=True)  88 us
    dot_general x3, matrix products, project_down(): jnp.dot(hidden, lax.all_gather(weight, 'fs', axis=1, tiled=True), preferr...  40.1 us
    all_gather x1, waiting for transfers between devices, mixer_inputs(): lax.all_gather(outer_gate, 'fs', axis=0, tiled=True)  37.7 us
    all_gather x1, waiting for transfers between devices, mixer_inputs(): lax.all_gather(inner_gate, 'fs', axis=0, tiled=True)  34.6 us
  transfers between devices with their start and end apart: 22, of which 21 were waited for; matrix products, arithmetic and copies ran while one was open for 6% of the time, Pallas kernels for 0%

profile of v1, /device:TPU:0, one launch (start us, length us, event | category | flops | bytes accessed | tf_op | source)
XLA Modules:
  0.0 855.2 jit_solution(7523875683802167748)
XLA Ops:
  6.5 0.7 all-gather.11.cloned.1.call-update
  7.3 0.0 all-gather.13.cloned.1.call-start
  7.3 0.7 all-gather.13.cloned.1.call-update
  8.0 0.0 all-gather.15.cloned.1.call-start
  8.1 0.7 all-gather.15.cloned.1.call-update
  8.7 0.0 reduce-scatter.4.cloned.1.call-start
  8.8 0.5 collective-permute-start
  9.3 11.8 %collective-permute-done = bf16[768,512]{1,0:T(8,128)(2,1)S(1)} collective-permute-done((bf16[768,512]{1,0:T(8,128)(2,1)}, bf16[768,512]{1,0:T(8,128)(2,1)S(1)}, u32[]{:S(2)}, u32[]{:S(2)}) %collective-permute-start) | collective-permute-done | bytes 786464 | tf_op jit(solution)/shard_map/ppermute | solution.py:15
  21.2 0.9 copy-done
  22.0 0.0 collective-permute-start.1
  22.1 11.4 %collective-permute-done.1 = bf16[768,512]{1,0:T(8,128)(2,1)S(1)} collective-permute-done((bf16[768,512]{1,0:T(8,128)(2,1)S(1)}, bf16[768,512]{1,0:T(8,128)(2,1)S(1)}, u32[]{:S(2)}, u32[]{:S(2)}) %collective-permute-start.1) | collective-permute-done | bytes 786464 | tf_op jit(solution)/shard_map/ppermute | solution.py:15
  33.5 0.9 copy-done.1
  34.3 10.6 %collective-permute-done.2 = bf16[768,512]{1,0:T(8,128)(2,1)} collective-permute-done((bf16[768,512]{1,0:T(8,128)(2,1)S(1)}, bf16[768,512]{1,0:T(8,128)(2,1)}, u32[]{:S(2)}, u32[]{:S(2)}) %collective-permute-start.2) | collective-permute-done | bytes 786464 | tf_op jit(solution)/shard_map/ppermute | solution.py:15
  45.0 7.9 fusion
  52.9 45.2 %all-gather.11.cloned.1.call-done = bf16[2048,1280]{1,0:T(8,128)(2,1)} async-done(((bf16[256,1280]{1,0:T(8,128)(2,1)}), bf16[2048,1280]{1,0:T(8,128)(2,1)}) %all-gather.11.cloned.1.call-update) | async-done | bytes 5242896 | tf_op jit(solution)/shard_map/all_gather | solution.py:41
  98.2 8.6 %fusion.39 = f32[768,1280]{1,0:T(8,128)} fusion(bf16[2048,1280]{1,0:T(8,128)(2,1)} %all-gather.11.cloned.1.call-done, bf16[768,2048]{1,0:T(8,128)(2,1)S(1)} %get-tuple-element.11, f32[2048]{0:T(1024)S(1)} %copy-done.3, f32[768]{0:T(1024)S(1)} %add_rsqrt_fusion.2), kind=kOutput, calls=%fused_computation.74 | convolution fusion | flops 4032823296 | bytes 12332032 | tf_op jit(solution)/shard_map/dot_general | solution.py:32
  106.8 77.6 %all-gather.13.cloned.1.call-done = bf16[2048,1280]{1,0:T(8,128)(2,1)} async-done(((bf16[256,1280]{1,0:T(8,128)(2,1)}), bf16[2048,1280]{1,0:T(8,128)(2,1)}) %all-gather.13.cloned.1.call-update) | async-done | bytes 5242896 | tf_op jit(solution)/shard_map/all_gather | solution.py:42
  184.4 87.0 %all-gather.15.cloned.1.call-done = bf16[1280,2048]{1,0:T(8,128)(2,1)} async-done(((bf16[1280,256]{1,0:T(8,128)(2,1)}), bf16[1280,2048]{1,0:T(8,128)(2,1)}) %all-gather.15.cloned.1.call-update) | async-done | bytes 5242896 | tf_op jit(solution)/shard_map/all_gather | solution.py:62
  271.5 16.4 %convolution_convert_fusion.2 = bf16[768,2048]{1,0:T(8,128)(2,1)} fusion(bf16[1280,2048]{1,0:T(8,128)(2,1)} %all-gather.15.cloned.1.call-done, bf16[2048,1280]{1,0:T(8,128)(2,1)} %all-gather.13.cloned.1.call-done, f32[768,1280]{1,0:T(8,128)} %fusion.39, bf16[768,2048]{1,0:T(8,128)(2,1)S(1)} %get-tuple-element.11, f32[2048]{0:T(1024)S(1)} %copy-done.3, ...), kind=kOutput, calls=%fused_computation.45 | convolution fusion | flops 8066826240 | bytes 20720640 | tf_op jit(solution)/shard_map/dot_general | solution.py:61
  287.9 0.0 all-gather.21.cloned.1.call-start
  288.0 0.5 all-gather.21.cloned.1.call-update
  288.5 0.0 all-gather.19.cloned.1.call-start
  288.5 0.5 all-gather.19.cloned.1.call-update
  289.1 0.0 all-gather.17.cloned.1.call-start
  289.1 34.8 %reduce-scatter.4.cloned.1.call-done = bf16[768,512]{1,0:T(8,128)(2,1)} async-done(((bf16[768,2048]{1,0:T(8,128)(2,1)}), bf16[768,512]{1,0:T(8,128)(2,1)}) %reduce-scatter.4.cloned.1.call-update) | async-done | bytes 786448 | tf_op jit(solution)/shard_map/reduce_scatter | solution.py:64
  324.0 1.6 add_convert_fusion.2
  325.6 0.1 collective-permute-start.3
  325.6 0.0 all-gather.17.cloned.1.call-update
  325.6 0.0 all-gather.23.cloned.1.call-start
  325.7 11.3 %collective-permute-done.3 = bf16[768,512]{1,0:T(8,128)(2,1)S(1)} collective-permute-done((bf16[768,512]{1,0:T(8,128)(2,1)S(1)}, bf16[768,512]{1,0:T(8,128)(2,1)S(1)}, u32[]{:S(2)}, u32[]{:S(2)}) %collective-permute-start.3) | collective-permute-done | bytes 786464 | tf_op jit(solution)/shard_map/ppermute | solution.py:15
  337.0 11.4 %collective-permute-done.4 = bf16[768,512]{1,0:T(8,128)(2,1)S(1)} collective-permute-done((bf16[768,512]{1,0:T(8,128)(2,1)S(1)}, bf16[768,512]{1,0:T(8,128)(2,1)S(1)}, u32[]{:S(2)}, u32[]{:S(2)}) %collective-permute-start.4) | collective-permute-done | bytes 786464 | tf_op jit(solution)/shard_map/ppermute | solution.py:15
  348.4 0.0 all-gather.23.cloned.1.call-update
  348.5 0.0 reduce-scatter.6.cloned.1.call-start
  348.5 11.3 %collective-permute-done.5 = bf16[768,512]{1,0:T(8,128)(2,1)S(1)} collective-permute-done((bf16[768,512]{1,0:T(8,128)(2,1)S(1)}, bf16[768,512]{1,0:T(8,128)(2,1)S(1)}, u32[]{:S(2)}, u32[]{:S(2)}) %collective-permute-start.5) | collective-permute-done | bytes 786464 | tf_op jit(solution)/shard_map/ppermute | solution.py:15
  359.9 9.5 %fusion.3 = (f32[768]{0:T(1024)S(1)}, bf16[768,2048]{1,0:T(8,128)(2,1)}) fusion(s32[]{:T(128)S(6)} %select_n.15, bf16[768,512]{1,0:T(8,128)(2,1)S(1)} %add_convert_fusion.2, bf16[768,512]{1,0:T(8,128)(2,1)S(1)} %collective-permute-done.3, bf16[768,512]{1,0:T(8,128)(2,1)S(1)} %collective-permute-done.4, bf16[768,512]{1,0:T(8,128)(2,1)S(1)} %collective-permute-done.5), kind=kLoop, calls=%fused_computation.9 | loop fusion | flops 29883648 | bytes 6294532 | tf_op jit(solution)/shard_map/reduce_sum | solution.py:27
  369.4 3.2 fusion.49
  372.6 34.6 %all-gather.19.cloned.1.call-done = bf16[2048,256]{1,0:T(8,128)(2,1)} async-done(((bf16[256,256]{1,0:T(8,128)(2,1)}), bf16[2048,256]{1,0:T(8,128)(2,1)}) %all-gather.19.cloned.1.call-update) | async-done | bytes 1048592 | tf_op jit(solution)/shard_map/all_gather | solution.py:56
  407.2 3.2 convolution_multiply_fusion.2
  410.4 0.2 fusion.45
  410.7 37.7 %all-gather.17.cloned.1.call-done = bf16[2048,256]{1,0:T(8,128)(2,1)} async-done(((bf16[256,256]{1,0:T(8,128)(2,1)}), bf16[2048,256]{1,0:T(8,128)(2,1)}) %all-gather.17.cloned.1.call-update) | async-done | bytes 1048592 | tf_op jit(solution)/shard_map/all_gather | solution.py:55
  448.4 40.2 %all-gather.23.cloned.1.call-done = bf16[256,2048]{1,0:T(8,128)(2,1)} async-done(((bf16[256,256]{1,0:T(8,128)(2,1)}), bf16[256,2048]{1,0:T(8,128)(2,1)}) %all-gather.23.cloned.1.call-update) | async-done | bytes 1048592 | tf_op jit(solution)/shard_map/all_gather | solution.py:62
  488.6 7.5 convolution_convert_fusion
  496.1 0.0 all-gather.25.cloned.1.call-start
  496.2 0.5 all-gather.25.cloned.1.call-update
  496.7 0.0 all-gather.27.cloned.1.call-start
  496.8 0.7 all-gather.27.cloned.1.call-update
  497.4 0.0 all-gather.29.cloned.1.call-start
  497.5 0.5 all-gather.29.cloned.1.call-update
  498.0 0.0 reduce-scatter.8.cloned.1.call-start
  498.1 34.9 %reduce-scatter.6.cloned.1.call-done = bf16[768,512]{1,0:T(8,128)(2,1)} async-done(((bf16[768,2048]{1,0:T(8,128)(2,1)}), bf16[768,512]{1,0:T(8,128)(2,1)}) %reduce-scatter.6.cloned.1.call-update) | async-done | bytes 786448 | tf_op jit(solution)/shard_map/reduce_scatter | solution.py:64
  533.0 1.3 add_convert_fusion.1
  534.3 0.1 collective-permute-start.6
  534.4 11.4 %collective-permute-done.6 = bf16[768,512]{1,0:T(8,128)(2,1)S(1)} collective-permute-done((bf16[768,512]{1,0:T(8,128)(2,1)S(1)}, bf16[768,512]{1,0:T(8,128)(2,1)S(1)}, u32[]{:S(2)}, u32[]{:S(2)}) %collective-permute-start.6) | collective-permute-done | bytes 786464 | tf_op jit(solution)/shard_map/ppermute | solution.py:15
  545.8 11.4 %collective-permute-done.7 = bf16[768,512]{1,0:T(8,128)(2,1)S(1)} collective-permute-done((bf16[768,512]{1,0:T(8,128)(2,1)S(1)}, bf16[768,512]{1,0:T(8,128)(2,1)S(1)}, u32[]{:S(2)}, u32[]{:S(2)}) %collective-permute-start.7) | collective-permute-done | bytes 786464 | tf_op jit(solution)/shard_map/ppermute | solution.py:15
  557.2 11.4 %collective-permute-done.8 = bf16[768,512]{1,0:T(8,128)(2,1)S(1)} collective-permute-done((bf16[768,512]{1,0:T(8,128)(2,1)S(1)}, bf16[768,512]{1,0:T(8,128)(2,1)S(1)}, u32[]{:S(2)}, u32[]{:S(2)}) %collective-permute-start.8) | collective-permute-done | bytes 786464 | tf_op jit(solution)/shard_map/ppermute | solution.py:15
  568.6 9.5 %fusion.6 = (f32[768]{0:T(1024)S(1)}, bf16[768,2048]{1,0:T(8,128)(2,1)}) fusion(s32[]{:T(128)S(6)} %select_n.15, bf16[768,512]{1,0:T(8,128)(2,1)S(1)} %add_convert_fusion.1, bf16[768,512]{1,0:T(8,128)(2,1)S(1)} %collective-permute-done.6, bf16[768,512]{1,0:T(8,128)(2,1)S(1)} %collective-permute-done.7, bf16[768,512]{1,0:T(8,128)(2,1)S(1)} %collective-permute-done.8), kind=kLoop, calls=%fused_computation.12 | loop fusion | flops 29883648 | bytes 6294532 | tf_op jit(solution)/shard_map/reduce_sum | solution.py:27
  578.2 42.8 %all-gather.25.cloned.1.call-done = bf16[2048,1280]{1,0:T(8,128)(2,1)} async-done(((bf16[256,1280]{1,0:T(8,128)(2,1)}), bf16[2048,1280]{1,0:T(8,128)(2,1)}) %all-gather.25.cloned.1.call-update) | async-done | bytes 5242896 | tf_op jit(solution)/shard_map/all_gather | solution.py:41
  621.0 9.6 %fusion.34 = f32[768,1280]{1,0:T(8,128)} fusion(bf16[2048,1280]{1,0:T(8,128)(2,1)} %all-gather.25.cloned.1.call-done, bf16[768,2048]{1,0:T(8,128)(2,1)} %get-tuple-element.7, f32[2048]{0:T(1024)S(1)} %copy-done.5, f32[768]{0:T(1024)S(1)} %add_rsqrt_fusion), kind=kOutput, calls=%fused_computation.73 | convolution fusion | flops 4032823296 | bytes 12332032 | tf_op jit(solution)/shard_map/dot_general | solution.py:32
  630.5 76.7 %all-gather.27.cloned.1.call-done = bf16[2048,1280]{1,0:T(8,128)(2,1)} async-done(((bf16[256,1280]{1,0:T(8,128)(2,1)}), bf16[2048,1280]{1,0:T(8,128)(2,1)}) %all-gather.27.cloned.1.call-update) | async-done | bytes 5242896 | tf_op jit(solution)/shard_map/all_gather | solution.py:42
  707.2 86.9 %all-gather.29.cloned.1.call-done = bf16[1280,2048]{1,0:T(8,128)(2,1)} async-done(((bf16[1280,256]{1,0:T(8,128)(2,1)}), bf16[1280,2048]{1,0:T(8,128)(2,1)}) %all-gather.29.cloned.1.call-update) | async-done | bytes 5242896 | tf_op jit(solution)/shard_map/all_gather | solution.py:62
  794.1 16.2 %convolution_convert_fusion.1 = bf16[768,2048]{1,0:T(8,128)(2,1)} fusion(bf16[1280,2048]{1,0:T(8,128)(2,1)} %all-gather.29.cloned.1.call-done, bf16[2048,1280]{1,0:T(8,128)(2,1)} %all-gather.27.cloned.1.call-done, f32[768,1280]{1,0:T(8,128)} %fusion.34, bf16[768,2048]{1,0:T(8,128)(2,1)} %get-tuple-element.7, f32[2048]{0:T(1024)S(1)} %copy-done.5, ...), kind=kOutput, calls=%fused_computation.44 | convolution fusion | flops 8066826240 | bytes 20720640 | tf_op jit(solution)/shard_map/dot_general | solution.py:61
  810.3 0.0 reduce-scatter.8.cloned.1.call-update
  810.4 36.1 %reduce-scatter.8.cloned.1.call-done = bf16[768,512]{1,0:T(8,128)(2,1)} async-done(((bf16[768,2048]{1,0:T(8,128)(2,1)}), bf16[768,512]{1,0:T(8,128)(2,1)}) %reduce-scatter.8.cloned.1.call-update) | async-done | bytes 786448 | tf_op jit(solution)/shard_map/reduce_scatter | solution.py:64
  846.4 2.2 add_convert_fusion
  (23 shorter events, 0.1 us)
Async XLA Ops:
  6.5 91.6 %copy-start.3 = (f32[2048]{0:T(1024)S(1)}, f32[2048]{0:T(1024)}, u32[]{:S(2)}) copy-start(f32[2048]{0:T(1024)} %param.18) | copy-start | bytes 24580
  6.5 91.6 %all-gather.11.cloned.1.call-start = ((), (), s32[]{:S(2)}) async-start(), calls=%async_computation.3 | async-start | bytes 5898240 | tf_op jit(solution)/shard_map/all_gather | solution.py:41
  7.3 177.2 %all-gather.13.cloned.1.call-start = ((), (), s32[]{:S(2)}) async-start(), calls=%async_computation.4 | async-start | bytes 5898240 | tf_op jit(solution)/shard_map/all_gather | solution.py:42
  8.0 263.5 %all-gather.15.cloned.1.call-start = ((), (), s32[]{:S(2)}) async-start(), calls=%async_computation.5 | async-start | bytes 5898240 | tf_op jit(solution)/shard_map/all_gather | solution.py:62
  8.7 315.2 %reduce-scatter.4.cloned.1.call-start = ((), (), s32[]{:S(2)}) async-start(), calls=%async_computation.6 | async-start | bytes 3932160 | tf_op jit(solution)/shard_map/reduce_scatter | solution.py:64
  8.8 12.4 %collective-permute-start = (bf16[768,512]{1,0:T(8,128)(2,1)}, bf16[768,512]{1,0:T(8,128)(2,1)S(1)}, u32[]{:S(2)}, u32[]{:S(2)}) collective-permute-start(bf16[768,512]{1,0:T(8,128)(2,1)} %bitcast.18), channel_id=1, source_target_pairs={{0,1},{1,2},{2,3},{3,0},{4,5},{5,6},{6,7},{7,4},{8,9},{9,10},{10,1... | collective-permute-start | bytes 2359304 | tf_op jit(solution)/shard_map/ppermute | solution.py:15
  21.2 0.9 copy-start
  22.0 11.4 %collective-permute-start.1 = (bf16[768,512]{1,0:T(8,128)(2,1)S(1)}, bf16[768,512]{1,0:T(8,128)(2,1)S(1)}, u32[]{:S(2)}, u32[]{:S(2)}) collective-permute-start(bf16[768,512]{1,0:T(8,128)(2,1)S(1)} %collective-permute-done), channel_id=1, source_target_pairs={{0,1},{1,2},{2,3},{3,0},{4,5},{5,6},{6,7},{7,4},{8,9},{9,10},{10,1... | collective-permute-start | bytes 2359304 | tf_op jit(solution)/shard_map/ppermute | solution.py:15
  33.5 0.9 copy-start.1
  33.5 11.5 %collective-permute-start.2 = (bf16[768,512]{1,0:T(8,128)(2,1)S(1)}, bf16[768,512]{1,0:T(8,128)(2,1)}, u32[]{:S(2)}, u32[]{:S(2)}) collective-permute-start(bf16[768,512]{1,0:T(8,128)(2,1)S(1)} %collective-permute-done.1), channel_id=1, source_target_pairs={{0,1},{1,2},{2,3},{3,0},{4,5},{5,6},{6,7},{7,4},{8,9},{9,10},{10,1... | collective-permute-start | bytes 2359304 | tf_op jit(solution)/shard_map/ppermute | solution.py:15
  287.9 60.6 %copy-start.2 = (f32[3,256]{1,0:T(4,128)S(1)}, f32[3,256]{1,0:T(4,128)}, u32[]{:S(2)}) copy-start(f32[3,256]{1,0:T(4,128)} %param.26) | copy-start | bytes 9220
  287.9 81.5 %copy-start.4 = (f32[2048]{0:T(1024)S(1)}, f32[2048]{0:T(1024)}, u32[]{:S(2)}) copy-start(f32[2048]{0:T(1024)} %param.22) | copy-start | bytes 24580
  287.9 81.5 %all-gather.21.cloned.1.call-start = ((), (), s32[]{:S(2)}) async-start(), calls=%async_computation.9 | async-start | bytes 1179648 | tf_op jit(solution)/shard_map/all_gather | solution.py:53
  288.5 118.7 %all-gather.19.cloned.1.call-start = ((), (), s32[]{:S(2)}) async-start(), calls=%async_computation.8 | async-start | bytes 1179648 | tf_op jit(solution)/shard_map/all_gather | solution.py:56
  289.1 159.3 %all-gather.17.cloned.1.call-start = ((), (), s32[]{:S(2)}) async-start(), calls=%async_computation.7 | async-start | bytes 1179648 | tf_op jit(solution)/shard_map/all_gather | solution.py:55
  325.6 11.5 %collective-permute-start.3 = (bf16[768,512]{1,0:T(8,128)(2,1)S(1)}, bf16[768,512]{1,0:T(8,128)(2,1)S(1)}, u32[]{:S(2)}, u32[]{:S(2)}) collective-permute-start(bf16[768,512]{1,0:T(8,128)(2,1)S(1)} %add_convert_fusion.2), channel_id=1, source_target_pairs={{0,1},{1,2},{2,3},{3,0},{4,5},{5,6},{6,7},{7,4},{8,9},{9,10},{10,1... | collective-permute-start | bytes 2359304 | tf_op jit(solution)/shard_map/ppermute | solution.py:15
  325.6 162.9 %all-gather.23.cloned.1.call-start = ((), (), s32[]{:S(2)}) async-start(), calls=%async_computation.10 | async-start | bytes 1179648 | tf_op jit(solution)/shard_map/all_gather | solution.py:62
  337.0 11.4 %collective-permute-start.4 = (bf16[768,512]{1,0:T(8,128)(2,1)S(1)}, bf16[768,512]{1,0:T(8,128)(2,1)S(1)}, u32[]{:S(2)}, u32[]{:S(2)}) collective-permute-start(bf16[768,512]{1,0:T(8,128)(2,1)S(1)} %collective-permute-done.3), channel_id=1, source_target_pairs={{0,1},{1,2},{2,3},{3,0},{4,5},{5,6},{6,7},{7,4},{8,9},{9,10},{10,1... | collective-permute-start | bytes 2359304 | tf_op jit(solution)/shard_map/ppermute | solution.py:15
  348.4 11.4 %collective-permute-start.5 = (bf16[768,512]{1,0:T(8,128)(2,1)S(1)}, bf16[768,512]{1,0:T(8,128)(2,1)S(1)}, u32[]{:S(2)}, u32[]{:S(2)}) collective-permute-start(bf16[768,512]{1,0:T(8,128)(2,1)S(1)} %collective-permute-done.4), channel_id=1, source_target_pairs={{0,1},{1,2},{2,3},{3,0},{4,5},{5,6},{6,7},{7,4},{8,9},{9,10},{10,1... | collective-permute-start | bytes 2359304 | tf_op jit(solution)/shard_map/ppermute | solution.py:15
  348.5 184.5 %reduce-scatter.6.cloned.1.call-start = ((), (), s32[]{:S(2)}) async-start(), calls=%async_computation.11 | async-start | bytes 3932160 | tf_op jit(solution)/shard_map/reduce_scatter | solution.py:64
  496.1 124.8 %copy-start.5 = (f32[2048]{0:T(1024)S(1)}, f32[2048]{0:T(1024)}, u32[]{:S(2)}) copy-start(f32[2048]{0:T(1024)} %param.28) | copy-start | bytes 24580
  496.1 124.8 %all-gather.25.cloned.1.call-start = ((), (), s32[]{:S(2)}) async-start(), calls=%async_computation.12 | async-start | bytes 5898240 | tf_op jit(solution)/shard_map/all_gather | solution.py:41
  496.7 210.5 %all-gather.27.cloned.1.call-start = ((), (), s32[]{:S(2)}) async-start(), calls=%async_computation.13 | async-start | bytes 5898240 | tf_op jit(solution)/shard_map/all_gather | solution.py:42
  497.4 296.7 %all-gather.29.cloned.1.call-start = ((), (), s32[]{:S(2)}) async-start(), calls=%async_computation.14 | async-start | bytes 5898240 | tf_op jit(solution)/shard_map/all_gather | solution.py:62
  498.0 348.4 %reduce-scatter.8.cloned.1.call-start = ((), (), s32[]{:S(2)}) async-start(), calls=%async_computation.15 | async-start | bytes 3932160 | tf_op jit(solution)/shard_map/reduce_scatter | solution.py:64
  534.3 11.5 %collective-permute-start.6 = (bf16[768,512]{1,0:T(8,128)(2,1)S(1)}, bf16[768,512]{1,0:T(8,128)(2,1)S(1)}, u32[]{:S(2)}, u32[]{:S(2)}) collective-permute-start(bf16[768,512]{1,0:T(8,128)(2,1)S(1)} %add_convert_fusion.1), channel_id=1, source_target_pairs={{0,1},{1,2},{2,3},{3,0},{4,5},{5,6},{6,7},{7,4},{8,9},{9,10},{10,1... | collective-permute-start | bytes 2359304 | tf_op jit(solution)/shard_map/ppermute | solution.py:15
  545.8 11.4 %collective-permute-start.7 = (bf16[768,512]{1,0:T(8,128)(2,1)S(1)}, bf16[768,512]{1,0:T(8,128)(2,1)S(1)}, u32[]{:S(2)}, u32[]{:S(2)}) collective-permute-start(bf16[768,512]{1,0:T(8,128)(2,1)S(1)} %collective-permute-done.6), channel_id=1, source_target_pairs={{0,1},{1,2},{2,3},{3,0},{4,5},{5,6},{6,7},{7,4},{8,9},{9,10},{10,1... | collective-permute-start | bytes 2359304 | tf_op jit(solution)/shard_map/ppermute | solution.py:15
  557.2 11.4 %collective-permute-start.8 = (bf16[768,512]{1,0:T(8,128)(2,1)S(1)}, bf16[768,512]{1,0:T(8,128)(2,1)S(1)}, u32[]{:S(2)}, u32[]{:S(2)}) collective-permute-start(bf16[768,512]{1,0:T(8,128)(2,1)S(1)} %collective-permute-done.7), channel_id=1, source_target_pairs={{0,1},{1,2},{2,3},{3,0},{4,5},{5,6},{6,7},{7,4},{8,9},{9,10},{10,1... | collective-permute-start | bytes 2359304 | tf_op jit(solution)/shard_map/ppermute | solution.py:15
Sparse Core Ops, SparseCore 0:
  9.5 88.5 all-gather.10
  100.3 84.0 all-gather.12
  186.5 84.9 all-gather.14
  288.0 35.8 reduce-scatter.3
  325.9 40.2 all-gather.20
  368.2 38.9 all-gather.18
  409.4 38.9 all-gather.16
  450.4 38.0 all-gather.22
  496.2 36.7 reduce-scatter.5
  535.0 85.8 all-gather.24
  623.1 84.0 all-gather.26
  709.1 84.9 all-gather.28
  810.5 35.8 reduce-scatter.7
